TPU v7x, 32 devices: a whole 2x2x4 slice. The times are simulated.
32 devices in a mesh: fs: 8 (over z, x), tp: 4 (over y, core).
Axes of the slice: x: 2, y: 2, z: 4, core: 2. Of those that a mesh axis runs over, the one named last changes fastest.
Arguments:
- q_latent: bfloat16 [6144, 512], P('fs'), may hold values from -6 to 6
- q_grad: bfloat16 [6144, 3072], P('fs', 'tp'), may hold values from -6 to 6
- uq_master: float32 [512, 3072], P('fs', 'tp'), may hold values from -6 to 6
- uq_basis: bfloat16 [512, 256], P('fs'), may hold values from -4 to 4
- uq_first: float32 [256, 3072], P('fs', 'tp'), may hold values from -3 to 3
- uq_second: float32 [256, 3072], P('fs', 'tp'), may hold values from 0.1 to 1
- kv_latent: bfloat16 [6144, 512], P('fs'), may hold values from -6 to 6
- k_grad: bfloat16 [6144, 2048], P('fs', 'tp'), may hold values from -6 to 6
- uk_master: float32 [512, 2048], P('fs', 'tp'), may hold values from -6 to 6
- uk_basis: bfloat16 [512, 256], P('fs'), may hold values from -4 to 4
- uk_first: float32 [256, 2048], P('fs', 'tp'), may hold values from -3 to 3
- uk_second: float32 [256, 2048], P('fs', 'tp'), may hold values from 0.1 to 1
Outputs:
- uq_first_new: float32 [256, 3072], P('fs', 'tp')
- uq_second_new: float32 [256, 3072], P('fs', 'tp')
- uq_step: float32 [512, 3072], P('fs', 'tp')
- uq_copy: bfloat16 [512, 3072], P(None, 'tp')
- uk_first_new: float32 [256, 2048], P('fs', 'tp')
- uk_second_new: float32 [256, 2048], P('fs', 'tp')
- uk_step: float32 [512, 2048], P('fs', 'tp')
- uk_copy: bfloat16 [512, 2048], P(None, 'tp')
All inputs are finite; a program needn't handle non-finite values.
Results may differ from a plain program's by a relative error of at most 0.0071.
Values may be sent and summed in bfloat16 or wider, within the bound.
A program may use at most 64 MiB of HBM per device.

v0:
```python
import jax
import jax.numpy as jnp
from jax import lax
from jax.sharding import PartitionSpec as P

first_decay = 0.8
second_decay = 0.9
step_size = 0.5
mean_guard = 1e-06
root_guard = 1e-08


def across_tokens(left, right):
    return lax.dot_general(
        left, right, (((0,), (0,)), ((), ())), preferred_element_type=jnp.float32
    )


def across_latent(left, right):
    return lax.dot_general(
        left,
        right,
        (((0,), (0,)), ((), ())),
        precision=lax.Precision.HIGHEST,
        preferred_element_type=jnp.float32,
    )


def moment_update(scaled, first_old, second_old):
    first_new = first_decay * first_old + (1.0 - first_decay) * scaled
    second_new = second_decay * second_old + (1.0 - second_decay) * scaled * scaled
    heading = (first_new / (jnp.sqrt(second_new) + root_guard)).astype(jnp.bfloat16)
    return (first_new, second_new, heading)


def body(
    q_latent,
    q_grad,
    uq_master,
    uq_basis,
    uq_first,
    uq_second,
    kv_latent,
    k_grad,
    uk_master,
    uk_basis,
    uk_first,
    uk_second,
):
    q_width = q_grad.shape[1]
    q_whole, k_whole = (
        lax.all_gather(uq_basis, "fs", axis=0, tiled=True),
        lax.all_gather(uk_basis, "fs", axis=0, tiled=True),
    )
    q_factor = q_whole.astype(jnp.float32)
    k_factor = k_whole.astype(jnp.float32)
    q_partial = across_tokens(q_latent, q_grad)
    k_partial = across_tokens(kv_latent, k_grad)
    projected = lax.psum_scatter(
        jnp.concatenate(
            [across_latent(q_factor, q_partial), across_latent(k_factor, k_partial)], axis=1
        ),
        "fs",
        scatter_dimension=0,
        tiled=True,
    )
    squares_sum = lax.psum(jnp.sum(projected * projected), ("fs", "tp"))
    entry_count = (
        projected.shape[0] * projected.shape[1] * lax.axis_size("fs") * lax.axis_size("tp")
    )
    root_mean = jnp.sqrt(squares_sum / entry_count + mean_guard)
    scaled = projected / root_mean
    uq_first_new, uq_second_new, q_heading = moment_update(scaled[:, :q_width], uq_first, uq_second)
    uk_first_new, uk_second_new, k_heading = moment_update(scaled[:, q_width:], uk_first, uk_second)
    q_dir, k_dir = (
        lax.all_gather(q_heading, "fs", axis=0, tiled=True),
        lax.all_gather(k_heading, "fs", axis=0, tiled=True),
    )
    uq_step = jnp.dot(uq_basis, q_dir, preferred_element_type=jnp.float32)
    uk_step = jnp.dot(uk_basis, k_dir, preferred_element_type=jnp.float32)
    q_fresh = (uq_master - step_size * uq_step).astype(jnp.bfloat16)
    k_fresh = (uk_master - step_size * uk_step).astype(jnp.bfloat16)
    uq_copy, uk_copy = (
        lax.all_gather(q_fresh, "fs", axis=0, tiled=True),
        lax.all_gather(k_fresh, "fs", axis=0, tiled=True),
    )
    return (
        uq_first_new,
        uq_second_new,
        uq_step,
        uq_copy,
        uk_first_new,
        uk_second_new,
        uk_step,
        uk_copy,
    )


def solution(mesh):
    return jax.shard_map(
        body,
        mesh=mesh,
        in_specs=(
            P("fs", None),
            P("fs", "tp"),
            P("fs", "tp"),
            P("fs", None),
            P("fs", "tp"),
            P("fs", "tp"),
            P("fs", None),
            P("fs", "tp"),
            P("fs", "tp"),
            P("fs", None),
            P("fs", "tp"),
            P("fs", "tp"),
        ),
        out_specs=(
            P("fs", "tp"),
            P("fs", "tp"),
            P("fs", "tp"),
            P(None, "tp"),
            P("fs", "tp"),
            P("fs", "tp"),
            P("fs", "tp"),
            P(None, "tp"),
        ),
        check_vma=False,
    )
```

profile of v0, /device:TPU:0, one launch (start us, length us, event | category | flops | bytes accessed | tf_op | source)
XLA Modules:
  0.0 323.5 jit_solution(11529704585300049106)
XLA Ops:
  7.2 0.0 reduce-scatter.4.cloned.1.call-start
  7.2 32.9 %all_gather.18 = bf16[512,256]{1,0:T(8,128)(2,1)S(1)} all-gather(bf16[64,256]{1,0:T(8,128)(2,1)} %param.15), channel_id=1, replica_groups=mesh['fs'=8,'tp'=4] {'fs'}, dimensions={0}, use_global_device_ids=true | all-gather | bytes 294912 | tf_op jit(solution)/shard_map/all_gather | solution.py:52
  40.2 30.9 %all_gather.19 = bf16[512,256]{1,0:T(8,128)(2,1)S(1)} all-gather(bf16[64,256]{1,0:T(8,128)(2,1)} %param.21), channel_id=1, replica_groups=mesh['fs'=8,'tp'=4] {'fs'}, dimensions={0}, use_global_device_ids=true | all-gather | bytes 294912 | tf_op jit(solution)/shard_map/all_gather | solution.py:53
  71.1 1.9 fusion.4
  73.1 1.4 convolution_bitcast_fusion
  74.5 0.6 fusion.5
  75.1 1.0 convolution_bitcast_fusion.1
  76.1 0.1 pad_maximum_fusion
  76.2 1.5 copy.39
  77.7 0.0 reduce-scatter.4.cloned.1.call-update
  77.8 66.1 %reduce-scatter.4.cloned.1.call-done = f32[32,1280]{1,0:T(8,128)} async-done(((f32[256,1280]{1,0:T(8,128)}), f32[32,1280]{1,0:T(8,128)}) %reduce-scatter.4.cloned.1.call-update) | async-done | bytes 163856 | tf_op jit(solution)/shard_map/reduce_scatter | solution.py:59
  143.9 1.2 copy.40
  145.1 0.8 multiply_reduce_fusion
  145.9 39.9 %psum.7 = f32[]{:T(128)} all-reduce(f32[]{:T(128)} %multiply_reduce_fusion), channel_id=1, replica_groups=mesh['fs'=8,'tp'=4] {'fs','tp'}, use_global_device_ids=true, to_apply=%region_2.0 | all-reduce | flops 1 | bytes 8 | tf_op jit(solution)/shard_map/psum | solution.py:67
  186.5 0.7 divide_convert_fusion
  187.3 31.3 %all_gather.20 = bf16[256,768]{1,0:T(8,128)(2,1)S(1)} all-gather(bf16[32,768]{1,0:T(8,128)(2,1)S(1)} %get-tuple-element.27), channel_id=1, replica_groups=mesh['fs'=8,'tp'=4] {'fs'}, dimensions={0}, use_global_device_ids=true | all-gather | bytes 442368 | tf_op jit(solution)/shard_map/all_gather | solution.py:76
  218.5 0.9 subtract_convert_fusion
  219.4 32.1 %all_gather.21 = bf16[512,768]{1,0:T(8,128)(2,1)S(1)} all-gather(bf16[64,768]{1,0:T(8,128)(2,1)S(1)} %get-tuple-element.30), channel_id=1, replica_groups=mesh['fs'=8,'tp'=4] {'fs'}, dimensions={0}, use_global_device_ids=true | all-gather | bytes 884736 | tf_op jit(solution)/shard_map/all_gather | solution.py:84
  251.5 0.7 divide_convert_fusion.1
  252.2 30.8 %all_gather.22 = bf16[256,512]{1,0:T(8,128)(2,1)S(1)} all-gather(bf16[32,512]{1,0:T(8,128)(2,1)S(1)} %get-tuple-element.24), channel_id=1, replica_groups=mesh['fs'=8,'tp'=4] {'fs'}, dimensions={0}, use_global_device_ids=true | all-gather | bytes 294912 | tf_op jit(solution)/shard_map/all_gather | solution.py:77
  283.0 0.8 subtract_convert_fusion.1
  283.8 31.2 %all_gather.23 = bf16[512,512]{1,0:T(8,128)(2,1)S(1)} all-gather(bf16[64,512]{1,0:T(8,128)(2,1)S(1)} %get-tuple-element.32), channel_id=1, replica_groups=mesh['fs'=8,'tp'=4] {'fs'}, dimensions={0}, use_global_device_ids=true | all-gather | bytes 589824 | tf_op jit(solution)/shard_map/all_gather | solution.py:85
  315.0 0.9 copy.43
  315.9 0.8 copy.44
  (25 shorter events, 0.1 us)
Async XLA Ops:
  7.2 63.9 %copy-start = (bf16[768,768]{1,0:T(8,128)(2,1)S(1)}, bf16[768,768]{1,0:T(8,128)(2,1)}, u32[]{:S(2)}) copy-start(bf16[768,768]{1,0:T(8,128)(2,1)} %param.13) | copy-start | bytes 3538948
  7.2 136.7 %reduce-scatter.4.cloned.1.call-start = ((), (), s32[]{:S(2)}) async-start(), calls=%async_computation.1 | async-start | bytes 1474560 | tf_op jit(solution)/shard_map/reduce_scatter | solution.py:59
  73.1 1.4 copy-start.1
  73.1 1.4 copy-start.2
  77.7 108.8 %copy-start.8 = (f32[32,768]{1,0:T(8,128)S(1)}, f32[32,768]{1,0:T(8,128)}, u32[]{:S(2)}) copy-start(f32[32,768]{1,0:T(8,128)} %param.17) | copy-start | bytes 294916
  77.7 108.8 %copy-start.9 = (f32[32,768]{1,0:T(8,128)S(1)}, f32[32,768]{1,0:T(8,128)}, u32[]{:S(2)}) copy-start(f32[32,768]{1,0:T(8,128)} %param.16) | copy-start | bytes 294916
  77.8 140.8 %copy-start.4 = (f32[64,768]{1,0:T(8,128)S(1)}, f32[64,768]{1,0:T(8,128)}, u32[]{:S(2)}) copy-start(f32[64,768]{1,0:T(8,128)} %param.14) | copy-start | bytes 589828
  77.8 140.7 %copy-start.6 = (bf16[64,256]{1,0:T(8,128)(2,1)S(1)}, bf16[64,256]{1,0:T(8,128)(2,1)}, u32[]{:S(2)}) copy-start(bf16[64,256]{1,0:T(8,128)(2,1)} %param.15) | copy-start | bytes 98308
  143.9 42.6 %copy-start.3 = (f32[32,1280]{1,0:T(8,128)S(1)}, f32[32,1280]{1,0:T(8,128)}, u32[]{:S(2)}) copy-start(f32[32,1280]{1,0:T(8,128)} %reduce-scatter.4.cloned.1.call-done) | copy-start | bytes 491524
  186.5 65.0 %copy-start.10 = (f32[32,512]{1,0:T(8,128)S(1)}, f32[32,512]{1,0:T(8,128)}, u32[]{:S(2)}) copy-start(f32[32,512]{1,0:T(8,128)} %param.23) | copy-start | bytes 196612
  186.5 65.0 %copy-start.11 = (f32[32,512]{1,0:T(8,128)S(1)}, f32[32,512]{1,0:T(8,128)}, u32[]{:S(2)}) copy-start(f32[32,512]{1,0:T(8,128)} %param.22) | copy-start | bytes 196612
  218.5 64.5 %copy-start.5 = (f32[64,512]{1,0:T(8,128)S(1)}, f32[64,512]{1,0:T(8,128)}, u32[]{:S(2)}) copy-start(f32[64,512]{1,0:T(8,128)} %param.20) | copy-start | bytes 393220
  218.5 64.5 %copy-start.7 = (bf16[64,256]{1,0:T(8,128)(2,1)S(1)}, bf16[64,256]{1,0:T(8,128)(2,1)}, u32[]{:S(2)}) copy-start(bf16[64,256]{1,0:T(8,128)(2,1)} %param.21) | copy-start | bytes 98308
Sparse Core Ops, SparseCore 0:
  77.9 65.9 reduce-scatter.3
where the time goes:
time: 324 us; the launch traced here: 323 us
  blocking collectives  229 us (71%)
  waiting for transfers between devices  66.1 us (20%)
  between operations  14.9 us (5%)
  matrix products  6.67 us (2%)
  local copies, waits for them, and re-layouts  4.45 us (1%)
    reduce_scatter x1, waiting for transfers between devices, body(): lax.psum_scatter(jnp.concatenate([across_latent(q_factor, q_partial), acr...  66.1 us
    psum x1, blocking collectives, body(): squares_sum = lax.psum(jnp.sum(projected * projected), ('fs', 'tp'))  39.9 us
    all_gather x1, blocking collectives, body(): lax.all_gather(uq_basis, 'fs', axis=0, tiled=True)  32.9 us
    all_gather x1, blocking collectives, body(): lax.all_gather(q_fresh, 'fs', axis=0, tiled=True)  32.1 us
    all_gather x1, blocking collectives, body(): lax.all_gather(q_heading, 'fs', axis=0, tiled=True)  31.3 us
    all_gather x1, blocking collectives, body(): lax.all_gather(k_fresh, 'fs', axis=0, tiled=True)  31.2 us
    all_gather x1, blocking collectives, body(): lax.all_gather(uk_basis, 'fs', axis=0, tiled=True)  30.9 us
    all_gather x1, blocking collectives, body(): lax.all_gather(k_heading, 'fs', axis=0, tiled=True)  30.8 us
  transfers between devices with their start and end apart: 1, of which 1 were waited for; matrix products, arithmetic and copies ran while one was open for 0% of the time, Pallas kernels for 0%

commit v1 on v0

--- a/solution.py
+++ b/solution.py
@@ -81,7 +81,9 @@
     q_fresh = (uq_master - step_size * uq_step).astype(jnp.bfloat16)
     k_fresh = (uk_master - step_size * uk_step).astype(jnp.bfloat16)
     uq_copy, uk_copy = (
-        lax.all_gather(q_fresh, "fs", axis=0, tiled=True),
+        jnp.concatenate(
+            lax.all_to_all(jnp.stack([q_fresh] * lax.axis_size("fs")), "fs", 0, 0), axis=0
+        ),
         lax.all_gather(k_fresh, "fs", axis=0, tiled=True),
     )
     return (

time: 324 us -> 303 us (0.935)
  blocking collectives: 229 us -> 203 us
  starting transfers between devices: 0.04 us -> 4.87 us
    all_gather x1 -> x0, blocking collectives: 32.1 us -> none  [body(): lax.all_gather(q_fresh, 'fs', axis=0, tiled=True)]
    all_gather x1, blocking collectives: 30.8 us -> 36.7 us  [body(): lax.all_gather(k_heading, 'fs', axis=0, tiled=True)]
    all_to_all x0 -> x1, starting transfers between devices: none -> 4.84 us  [body(): lax.all_to_all(jnp.stack([q_fresh] * lax.axis_size('fs')), 'fs', 0, 0)]
  transfers between devices with their start and end apart: 1 -> 2, of which waited for: 1 -> 1; matrix products, arithmetic and copies ran while one was open for 0% -> 0% of each run, Pallas kernels for 0% -> 0%
where the time goes in v1:
time: 303 us
  blocking collectives  203 us (67%)
  waiting for transfers between devices  66.1 us (22%)
  between operations  14.9 us (5%)
  matrix products  6.67 us (2%)
  local copies, waits for them, and re-layouts  5.37 us (2%)
  starting transfers between devices  4.87 us (2%)
    reduce_scatter x1, waiting for transfers between devices, body(): lax.psum_scatter(jnp.concatenate([across_latent(q_factor, q_partial), acr...  66.1 us
    psum x1, blocking collectives, body(): squares_sum = lax.psum(jnp.sum(projected * projected), ('fs', 'tp'))  39.9 us
    all_gather x1, blocking collectives, body(): lax.all_gather(k_heading, 'fs', axis=0, tiled=True)  36.7 us
    all_gather x1, blocking collectives, body(): lax.all_gather(uq_basis, 'fs', axis=0, tiled=True)  32.9 us
    all_gather x1, blocking collectives, body(): lax.all_gather(k_fresh, 'fs', axis=0, tiled=True)  31.2 us
    all_gather x1, blocking collectives, body(): lax.all_gather(q_heading, 'fs', axis=0, tiled=True)  31.1 us
    all_gather x1, blocking collectives, body(): lax.all_gather(uk_basis, 'fs', axis=0, tiled=True)  30.9 us
  transfers between devices with their start and end apart: 2, of which 1 were waited for; matrix products, arithmetic and copies ran while one was open for 0% of the time, Pallas kernels for 0%

profile of v1, /device:TPU:0, one launch (start us, length us, event | category | flops | bytes accessed | tf_op | source)
XLA Modules:
  0.0 302.9 jit_solution(11147435918126866694)
XLA Ops:
  7.2 0.0 reduce-scatter.4.cloned.1.call-start
  7.2 32.9 %all_gather.15 = bf16[512,256]{1,0:T(8,128)(2,1)S(1)} all-gather(bf16[64,256]{1,0:T(8,128)(2,1)} %param.15), channel_id=1, replica_groups=mesh['fs'=8,'tp'=4] {'fs'}, dimensions={0}, use_global_device_ids=true | all-gather | bytes 294912 | tf_op jit(solution)/shard_map/all_gather | solution.py:52
  40.2 30.9 %all_gather.16 = bf16[512,256]{1,0:T(8,128)(2,1)S(1)} all-gather(bf16[64,256]{1,0:T(8,128)(2,1)} %param.21), channel_id=1, replica_groups=mesh['fs'=8,'tp'=4] {'fs'}, dimensions={0}, use_global_device_ids=true | all-gather | bytes 294912 | tf_op jit(solution)/shard_map/all_gather | solution.py:53
  71.1 1.9 fusion.4
  73.1 1.4 convolution_bitcast_fusion
  74.5 0.6 fusion.5
  75.1 1.0 convolution_bitcast_fusion.1
  76.1 0.1 pad_maximum_fusion
  76.2 1.5 copy.39
  77.8 66.1 %reduce-scatter.4.cloned.1.call-done = f32[32,1280]{1,0:T(8,128)} async-done(((f32[256,1280]{1,0:T(8,128)}), f32[32,1280]{1,0:T(8,128)}) %reduce-scatter.4.cloned.1.call-update) | async-done | bytes 163856 | tf_op jit(solution)/shard_map/reduce_scatter | solution.py:59
  143.9 1.2 copy.40
  145.1 0.8 multiply_reduce_fusion
  145.9 39.9 %psum.7 = f32[]{:T(128)} all-reduce(f32[]{:T(128)} %multiply_reduce_fusion), channel_id=1, replica_groups=mesh['fs'=8,'tp'=4] {'fs','tp'}, use_global_device_ids=true, to_apply=%region_2.0 | all-reduce | flops 1 | bytes 8 | tf_op jit(solution)/shard_map/psum | solution.py:67
  186.5 0.7 divide_convert_fusion
  187.2 31.1 %all_gather.17 = bf16[256,768]{1,0:T(8,128)(2,1)S(1)} all-gather(bf16[32,768]{1,0:T(8,128)(2,1)S(1)} %get-tuple-element.27), channel_id=1, replica_groups=mesh['fs'=8,'tp'=4] {'fs'}, dimensions={0}, use_global_device_ids=true | all-gather | bytes 442368 | tf_op jit(solution)/shard_map/all_gather | solution.py:76
  218.3 0.9 subtract_convert_fusion
  219.2 0.9 stack.2
  220.1 4.8 %all-to-all-start = ((bf16[8,64,768]{2,1,0:T(8,128)(2,1)}), bf16[8,64,768]{2,1,0:T(8,128)(2,1)S(1)}, u32[]{:S(2)}, u32[]{:S(2)}) async-start(bf16[8,64,768]{2,1,0:T(8,128)(2,1)} %stack.2), calls=%async_computation | async-start | bytes 1572864 | tf_op jit(solution)/shard_map/all_to_all | solution.py:85
  225.0 0.7 divide_convert_fusion.1
  225.7 36.7 %all_gather.18 = bf16[256,512]{1,0:T(8,128)(2,1)S(1)} all-gather(bf16[32,512]{1,0:T(8,128)(2,1)S(1)} %get-tuple-element.24), channel_id=1, replica_groups=mesh['fs'=8,'tp'=4] {'fs'}, dimensions={0}, use_global_device_ids=true | all-gather | bytes 294912 | tf_op jit(solution)/shard_map/all_gather | solution.py:77
  262.4 0.8 subtract_convert_fusion.1
  263.2 31.2 %all_gather.19 = bf16[512,512]{1,0:T(8,128)(2,1)S(1)} all-gather(bf16[64,512]{1,0:T(8,128)(2,1)S(1)} %get-tuple-element.32), channel_id=1, replica_groups=mesh['fs'=8,'tp'=4] {'fs'}, dimensions={0}, use_global_device_ids=true | all-gather | bytes 589824 | tf_op jit(solution)/shard_map/all_gather | solution.py:87
  294.3 0.9 copy.43
  295.2 0.8 copy.44
  (27 shorter events, 0.1 us)
Async XLA Ops:
  7.2 63.9 %copy-start = (bf16[768,768]{1,0:T(8,128)(2,1)S(1)}, bf16[768,768]{1,0:T(8,128)(2,1)}, u32[]{:S(2)}) copy-start(bf16[768,768]{1,0:T(8,128)(2,1)} %param.13) | copy-start | bytes 3538948
  7.2 136.7 %reduce-scatter.4.cloned.1.call-start = ((), (), s32[]{:S(2)}) async-start(), calls=%async_computation.2 | async-start | bytes 1474560 | tf_op jit(solution)/shard_map/reduce_scatter | solution.py:59
  73.1 1.4 copy-start.1
  73.1 1.4 copy-start.2
  77.7 108.7 %copy-start.8 = (f32[32,768]{1,0:T(8,128)S(1)}, f32[32,768]{1,0:T(8,128)}, u32[]{:S(2)}) copy-start(f32[32,768]{1,0:T(8,128)} %param.17) | copy-start | bytes 294916
  77.7 108.8 %copy-start.9 = (f32[32,768]{1,0:T(8,128)S(1)}, f32[32,768]{1,0:T(8,128)}, u32[]{:S(2)}) copy-start(f32[32,768]{1,0:T(8,128)} %param.16) | copy-start | bytes 294916
  77.8 140.5 %copy-start.4 = (f32[64,768]{1,0:T(8,128)S(1)}, f32[64,768]{1,0:T(8,128)}, u32[]{:S(2)}) copy-start(f32[64,768]{1,0:T(8,128)} %param.14) | copy-start | bytes 589828
  77.8 140.5 %copy-start.6 = (bf16[64,256]{1,0:T(8,128)(2,1)S(1)}, bf16[64,256]{1,0:T(8,128)(2,1)}, u32[]{:S(2)}) copy-start(bf16[64,256]{1,0:T(8,128)(2,1)} %param.15) | copy-start | bytes 98308
  143.9 42.6 %copy-start.3 = (f32[32,1280]{1,0:T(8,128)S(1)}, f32[32,1280]{1,0:T(8,128)}, u32[]{:S(2)}) copy-start(f32[32,1280]{1,0:T(8,128)} %reduce-scatter.4.cloned.1.call-done) | copy-start | bytes 491524
  219.2 5.8 %copy-start.10 = (f32[32,512]{1,0:T(8,128)S(1)}, f32[32,512]{1,0:T(8,128)}, u32[]{:S(2)}) copy-start(f32[32,512]{1,0:T(8,128)} %param.23) | copy-start | bytes 196612
  219.2 5.8 %copy-start.11 = (f32[32,512]{1,0:T(8,128)S(1)}, f32[32,512]{1,0:T(8,128)}, u32[]{:S(2)}) copy-start(f32[32,512]{1,0:T(8,128)} %param.22) | copy-start | bytes 196612
  220.1 42.2 %copy-start.5 = (f32[64,512]{1,0:T(8,128)S(1)}, f32[64,512]{1,0:T(8,128)}, u32[]{:S(2)}) copy-start(f32[64,512]{1,0:T(8,128)} %param.20) | copy-start | bytes 393220
  220.1 42.2 %copy-start.7 = (bf16[64,256]{1,0:T(8,128)(2,1)S(1)}, bf16[64,256]{1,0:T(8,128)(2,1)}, u32[]{:S(2)}) copy-start(bf16[64,256]{1,0:T(8,128)(2,1)} %param.21) | copy-start | bytes 98308
  220.1 74.2 %all-to-all-start = ((bf16[8,64,768]{2,1,0:T(8,128)(2,1)}), bf16[8,64,768]{2,1,0:T(8,128)(2,1)S(1)}, u32[]{:S(2)}, u32[]{:S(2)}) async-start(bf16[8,64,768]{2,1,0:T(8,128)(2,1)} %stack.2), calls=%async_computation | async-start | bytes 1572864 | tf_op jit(solution)/shard_map/all_to_all | solution.py:85
Sparse Core Ops, SparseCore 0:
  77.9 65.9 reduce-scatter.3
